TPU v7x, 32 devices: a whole 2x2x4 slice. The times are simulated.
32 devices in a mesh: sp: 8 (over z, y), dp: 4 (over x, core).
Axes of the slice: x: 2, y: 2, z: 4, core: 2. Of those that a mesh axis runs over, the one named last changes fastest.
Arguments:
- stream: bfloat16 [4, 1024, 2048], P('dp', 'sp'), may hold values from -6 to 6
- query_proj: bfloat16 [4, 1024, 2048], P('dp', 'sp'), may hold values from -6 to 6
- key_proj: bfloat16 [4, 1024, 2048], P('dp', 'sp'), may hold values from -6 to 6
- value_proj: bfloat16 [4, 1024, 2048], P('dp', 'sp'), may hold values from -6 to 6
- out_gate: bfloat16 [4, 1024, 2048], P('dp', 'sp'), may hold values from -6 to 6
- beta_logit: bfloat16 [4, 1024, 16], P('dp', 'sp'), may hold values from -6 to 6
- log_decay: float32 [4, 16, 1024], P('dp', 'sp'), may hold values from -0.8 to 0, as said below
- head_gain: float32 [128], replicated, may hold values from 0.1 to 1.9
- out_proj: bfloat16 [2048, 2048], replicated, may hold values from -0.125 to 0.125
- ffn_gain: float32 [2048], replicated, may hold values from 0.1 to 1.9
- routes: int32 [4, 1024, 2], P('dp', 'sp'), may hold values from 0 to 7, all different within a row; in each aligned block of 128 rows (0 to 127, 128 to 255, ..., all dimensions but the last counted through in order) at most 64 rows name the same one
- route_weight: float32 [4, 1024, 2], P('dp', 'sp'), may hold values from 0.1 to 1
- expert_gate: bfloat16 [8, 2048, 5120], P('sp', None, 'dp'), may hold values from -0.125 to 0.125
- expert_up: bfloat16 [8, 2048, 5120], P('sp', None, 'dp'), may hold values from -0.125 to 0.125
- expert_down: bfloat16 [8, 5120, 2048], P('sp', 'dp'), may hold values from -0.078125 to 0.078125
Outputs:
- result: bfloat16 [4, 1024, 2048], P('dp', 'sp')
Inputs may be any that keep to these rules, and one draw needn't show every extreme that they name: `routes`: each row names 2 different experts; within the rows of one device no expert is named more than 64 times, and some devices reach 64. log_decay is never positive.
All inputs are finite; a program needn't handle non-finite values.
Results may differ from a plain program's by a relative error of at most 0.0085.
Values may be sent and summed in bfloat16 or wider, within the bound.
A program may use at most 128 MiB of HBM per device.

v0:
```python
import jax
import jax.numpy as jnp
from jax import lax
from jax.sharding import PartitionSpec as P

HEAD_DIM = 128
BLOCK_LEN = 64


EPSILON = 1e-06
TOP_PRECISION = lax.Precision.HIGHEST


def unit_rows(matrix):
    return matrix * lax.rsqrt(jnp.sum(matrix * matrix, axis=-1, keepdims=True) + EPSILON)


def delta_blocks(queries, key_rows, values_in, log_rate, strength):
    length, n_heads, key_dim = key_rows.shape
    n_blocks = length // BLOCK_LEN

    def blocked(tensor):
        return tensor.reshape(n_blocks, BLOCK_LEN, n_heads, -1).transpose(0, 2, 1, 3)

    query_blk, key_blk, value_blk = (blocked(queries), blocked(key_rows), blocked(values_in))
    cumulative = jnp.cumsum(
        log_rate.reshape(n_blocks, BLOCK_LEN, n_heads).transpose(0, 2, 1), axis=-1
    )
    beta_blk = strength.reshape(n_blocks, BLOCK_LEN, n_heads).transpose(0, 2, 1)
    rows_idx = lax.broadcasted_iota(jnp.int32, (BLOCK_LEN, BLOCK_LEN), 0)
    cols_idx = lax.broadcasted_iota(jnp.int32, (BLOCK_LEN, BLOCK_LEN), 1)
    below_incl = rows_idx >= cols_idx
    strict = rows_idx > cols_idx
    decay_mat = jnp.exp(
        jnp.where(below_incl, cumulative[..., :, None] - cumulative[..., None, :], -jnp.inf)
    )
    key_beta = key_blk * beta_blk[..., None]
    lower_mat = jnp.where(
        strict,
        jnp.einsum("nhid,nhjd->nhij", key_beta, key_blk, precision=TOP_PRECISION) * decay_mat,
        0.0,
    )
    system = jnp.eye(BLOCK_LEN, dtype=jnp.float32) + lower_mat
    rhs_cols = jnp.concatenate(
        [value_blk * beta_blk[..., None], key_beta * jnp.exp(cumulative)[..., None]], axis=-1
    )
    solved = jax.scipy.linalg.solve_triangular(system, rhs_cols, lower=True, unit_diagonal=True)
    value_dim = value_blk.shape[-1]
    update, weight = (solved[..., :value_dim], solved[..., value_dim:])
    inside = jnp.einsum("nhid,nhjd->nhij", query_blk, key_blk, precision=TOP_PRECISION) * decay_mat

    def advance(running_state, inputs):
        query_inner, key_i, update_inner, weight_inner, running_total_inner, inside_i = inputs
        incoming_values = update_inner - jnp.einsum(
            "nli,nif->nlf", weight_inner, running_state, precision=TOP_PRECISION
        )
        result = jnp.einsum(
            "nli,nif->nlf",
            query_inner * jnp.exp(running_total_inner)[..., None],
            running_state,
            precision=TOP_PRECISION,
        )
        result = result + jnp.einsum(
            "hij,hjv->hiv", inside_i, incoming_values, precision=TOP_PRECISION
        )
        final_running_total = running_total_inner[:, -1:]
        trailing_key = key_i * jnp.exp(final_running_total - running_total_inner)[..., None]
        running_state = running_state * jnp.exp(final_running_total)[..., None] + jnp.einsum(
            "gbj,gbs->gjs", trailing_key, incoming_values, precision=TOP_PRECISION
        )
        return (running_state, result)

    zero_state = jnp.zeros((n_heads, key_dim, value_dim), jnp.float32)
    _, results = lax.scan(
        advance, zero_state, (query_blk, key_blk, update, weight, cumulative, inside)
    )
    return results.transpose(0, 2, 1, 3).reshape(length, n_heads, value_dim)


def mix_sequence(query_in, key_in, value_in, beta_in, decay_in):
    length = query_in.shape[0]
    n_heads = beta_in.shape[1]
    queries = unit_rows(
        query_in.reshape(length, n_heads, HEAD_DIM).astype(jnp.float32)
    ) * HEAD_DIM ** (-0.5)
    key_rows = unit_rows(key_in.reshape(length, n_heads, HEAD_DIM).astype(jnp.float32))
    values_in = value_in.reshape(length, n_heads, HEAD_DIM).astype(jnp.float32)
    strength = jax.nn.sigmoid(beta_in.astype(jnp.float32))
    log_rate = decay_in.T

    def two_ways(tensor):
        return jnp.concatenate([tensor, tensor[::-1]], axis=1)

    reads = delta_blocks(
        two_ways(queries),
        two_ways(key_rows),
        two_ways(values_in),
        two_ways(log_rate),
        two_ways(strength),
    )
    summed = reads[:, :n_heads] + reads[::-1, n_heads:]
    return summed.astype(jnp.bfloat16).reshape(length, n_heads * HEAD_DIM)


def expert_part(rows, gate_local, up_local, down_local):
    gate_act = jnp.dot(rows, gate_local, preferred_element_type=jnp.float32)
    up_act = jnp.dot(rows, up_local, preferred_element_type=jnp.float32)
    hidden = (jax.nn.silu(gate_act) * up_act).astype(jnp.bfloat16)
    return jnp.dot(hidden, down_local, preferred_element_type=jnp.float32)


def body(
    stream,
    query_proj,
    key_proj,
    value_proj,
    out_gate,
    beta_logit,
    log_decay,
    head_gain,
    out_proj,
    ffn_gain,
    routes,
    route_weight,
    expert_gate,
    expert_up,
    expert_down,
):
    heads_view = (
        lax.all_to_all(query_proj, "sp", split_axis=2, concat_axis=1, tiled=True),
        lax.all_to_all(key_proj, "sp", split_axis=2, concat_axis=1, tiled=True),
        lax.all_to_all(value_proj, "sp", split_axis=2, concat_axis=1, tiled=True),
        lax.all_to_all(beta_logit, "sp", split_axis=2, concat_axis=1, tiled=True),
    )
    mixed = mix_sequence(
        heads_view[0][0], heads_view[1][0], heads_view[2][0], heads_view[3][0], log_decay[0]
    )
    tokens_view = lax.all_to_all(mixed[None], "sp", split_axis=1, concat_axis=2, tiled=True)[0]
    tok_count = stream.shape[1]
    model_width = stream.shape[2]
    n_heads = tokens_view.shape[1] // HEAD_DIM
    per_head = tokens_view.astype(jnp.float32).reshape(tok_count, n_heads, HEAD_DIM)
    normed_heads = (
        per_head
        * lax.rsqrt(jnp.mean(per_head * per_head, axis=-1, keepdims=True) + EPSILON)
        * head_gain
    )
    gated = (
        normed_heads.reshape(tok_count, -1) * jax.nn.silu(out_gate[0].astype(jnp.float32))
    ).astype(jnp.bfloat16)
    resid = stream[0].astype(jnp.float32) + jnp.dot(
        gated, out_proj, preferred_element_type=jnp.float32
    )
    ffn_in = (
        resid * lax.rsqrt(jnp.mean(resid * resid, axis=-1, keepdims=True) + EPSILON) * ffn_gain
    ).astype(jnp.bfloat16)
    n_sp = lax.axis_size("sp")
    top_count = routes.shape[2]
    capacity = tok_count * top_count * 2 // n_sp
    flat_routes = routes.reshape(-1)
    expert_ids = lax.broadcasted_iota(jnp.int32, (1, n_sp), 1)
    chosen = (flat_routes[:, None] == expert_ids).astype(jnp.int32)
    earlier = jnp.cumsum(chosen, axis=0) - chosen
    slot_ids = flat_routes * capacity + jnp.sum(earlier * chosen, axis=1)
    slot_grid = lax.broadcasted_iota(jnp.int32, (n_sp * capacity, 1), 0)
    placing = (
        (slot_grid == slot_ids[None, :])
        .astype(jnp.int32)
        .reshape(n_sp * capacity, tok_count, top_count)
    )
    placing = jnp.sum(placing, axis=2).astype(jnp.bfloat16)
    outgoing = jnp.dot(placing, ffn_in, preferred_element_type=jnp.float32).astype(jnp.bfloat16)
    outgoing = outgoing.reshape(n_sp, capacity, model_width)
    gate_local = expert_gate[0]
    up_local = expert_up[0]
    down_local = expert_down[0]
    arrived = lax.all_to_all(outgoing, "sp", split_axis=0, concat_axis=0, tiled=True)
    piece = lax.all_gather(arrived, "dp", axis=0, tiled=True)
    flat_rows = piece.reshape(-1, model_width)
    partial_value = expert_part(flat_rows, gate_local, up_local, down_local).reshape(
        piece.shape[0], piece.shape[1], model_width
    )
    summed = lax.psum_scatter(
        partial_value.astype(jnp.bfloat16), "dp", scatter_dimension=0, tiled=True
    )
    returned = lax.all_to_all(summed, "sp", split_axis=0, concat_axis=0, tiled=True)
    picked = returned.reshape(n_sp * capacity, model_width)[slot_ids]
    picked = picked.reshape(tok_count, top_count, model_width).astype(jnp.float32)
    routed = jnp.sum(picked * route_weight[0][..., None], axis=1)
    return (resid + routed).astype(jnp.bfloat16)[None]


def solution(mesh):
    return jax.shard_map(
        body,
        mesh=mesh,
        in_specs=(
            P("dp", "sp", None),
            P("dp", "sp", None),
            P("dp", "sp", None),
            P("dp", "sp", None),
            P("dp", "sp", None),
            P("dp", "sp", None),
            P("dp", "sp", None),
            P(),
            P(),
            P(),
            P("dp", "sp", None),
            P("dp", "sp", None),
            P("sp", None, "dp"),
            P("sp", None, "dp"),
            P("sp", "dp", None),
        ),
        out_specs=P("dp", "sp", None),
        check_vma=False,
    )
```

profile of v0, /device:TPU:13, one launch (start us, length us, event | category | flops | bytes accessed | tf_op | source)
XLA Modules:
  0.0 910.8 jit_solution(16039289212015381199)
XLA Ops:
  7.8 5.7 all-to-all-start.1
  16.5 11.6 %reduce.7 = bf16[2048,128]{1,0:T(8,128)(2,1)S(1)} reduce(bf16[2048,1,128]{2,1,0:T(2,128)(2,1)S(1)} %bitcast.202, bf16[]{:T(256)} %broadcast.176), dimensions={1}, to_apply=%bitcast.144.reduce_sub_computation | reduce | bytes 1048578
  28.9 6.0 all-to-all-start
  39.0 11.6 %reduce.8 = bf16[2048,128]{1,0:T(8,128)(2,1)S(1)} reduce(bf16[2048,1,128]{2,1,0:T(2,128)(2,1)S(1)} %bitcast.212, bf16[]{:T(256)} %broadcast.176), dimensions={1}, to_apply=%bitcast.148.reduce_sub_computation | reduce | bytes 1048578
  52.3 11.6 %reduce.6 = bf16[2048,128]{1,0:T(8,128)(2,1)S(1)} reduce(bf16[2048,1,128]{2,1,0:T(2,128)(2,1)S(1)} %bitcast.213, bf16[]{:T(256)} %broadcast.176), dimensions={1}, to_apply=%bitcast.150.reduce_sub_computation | reduce | bytes 1048578
  67.7 5.6 all-to-all-start.2
  77.4 7.2 all-to-all-done.2
  84.7 6.1 all-to-all-start.3
  102.1 6.0 rev.21
  108.1 2.9 pad_maximum_fusion.1
  111.0 2.9 copy.187
  122.0 9.5 %reverse.8 = f32[1024,2,128]{0,2,1:T(8,128)} reverse(f32[1024,2,128]{0,2,1:T(8,128)} %get-tuple-element.169), dimensions={0} | reverse | bytes 2097152 | tf_op jit(solution)/shard_map/reverse
  134.3 2.9 copy.193
  137.2 4.5 copy_bitcast_fusion
  141.7 4.8 fusion.34
  146.6 5.2 add_bitcast_fusion
  151.8 316.0 %custom-call.4 = f32[16,4,1,64,64]{3,4,2,1,0:T(8,128)} custom-call(f32[16,4,1,64,64]{4,3,2,1,0:T(8,128)} %add_bitcast_fusion), custom_call_target="InvertDiagBlocksLowerTriangular" | custom-call | tf_op jit(solution)/shard_map/jit(_solve_triangular)/vmap(vmap())/triangular_solve | solution.py:47
  470.7 4.2 fusion.27
  476.8 100.8 %while.13 = (s32[]{:T(128)}, f32[4,128,128]{2,1,0:T(8,128)S(1)}, f32[16,4,64,128]{3,2,0,1:T(8,128)}, f32[16,4,64]{2,1,0:T(4,128)S(1)}, f32[16,4,64,128]{3,2,1,0:...) while((s32[]{:T(128)}, f32[4,128,128]{2,1,0:T(8,128)S(1)}, ...), condition=%wide.region_4.5_spmd.clone, body=%wide.region_3.4_spmd.clone.sunk | while | flops 176619776 | bytes 2500813 | solution.py:74
  581.9 4.0 reduce.9
  586.8 5.4 all-to-all-start.4
  593.9 9.4 %all-to-all-done.4 = bf16[8,2,16384]{2,1,0:T(2,128)(2,1)S(1)} async-done(((bf16[8,2,16384]{2,1,0:T(2,128)(2,1)}), bf16[8,2,16384]{2,1,0:T(2,128)(2,1)S(1)}, u32[]{:S(2)}, u32[]{:S(2)}) %all-to-all-start.4) | async-done | bytes 524320 | tf_op jit(solution)/shard_map/all_to_all | solution.py:138
  605.9 4.8 multiply_reduce_fusion.1
  611.5 51.1 %all_to_all.55 = bf16[8,64,2048]{2,1,0:T(8,128)(2,1)} all-to-all(bf16[8,64,2048]{2,1,0:T(8,128)(2,1)S(1)} %bitcast.199), channel_id=1, replica_groups=mesh['sp'=8,'dp'=4] {'sp'}, dimensions={0} | all-to-all | bytes 4194304 | tf_op jit(solution)/shard_map/all_to_all | solution.py:177
  662.6 61.2 %all-gather.2.cloned.1.call-done = bf16[32,64,2048]{2,1,0:T(8,128)(2,1)} async-done(((bf16[8,64,2048]{2,1,0:T(8,128)(2,1)}), bf16[32,64,2048]{2,1,0:T(8,128)(2,1)}) %all-gather.2.cloned.1.call-update) | async-done | bytes 8388624 | tf_op jit(solution)/shard_map/all_gather | solution.py:178
  723.8 16.7 %fusion.25 = f32[2048,1280]{1,0:T(8,128)} fusion(bf16[2048,2048]{1,0:T(8,128)(2,1)} %bitcast.229, bf16[1,2048,1280]{2,1,0:T(8,128)(2,1)} %param.29), kind=kOutput, calls=%fused_computation.37 | convolution fusion | flops 10737418240 | bytes 24117248 | tf_op jit(solution)/shard_map/dot_general | solution.py:106
  740.5 16.4 %multiply_convert_fusion = bf16[2048,1280]{1,0:T(8,128)(2,1)} fusion(f32[2048,1280]{1,0:T(8,128)} %fusion.25, bf16[2048,2048]{1,0:T(8,128)(2,1)S(1)} %bitcast.230, bf16[1,2048,1280]{2,1,0:T(8,128)(2,1)} %param.30), kind=kOutput, calls=%fused_computation.33 | convolution fusion | flops 10753146880 | bytes 29360128 | tf_op jit(solution)/shard_map/dot_general | solution.py:107
  756.9 15.5 %convolution_convert_fusion = bf16[32,64,2048]{2,1,0:T(8,128)(2,1)} fusion(bf16[32,64,1280]{2,1,0:T(8,128)(2,1)} %bitcast.233, bf16[1,1280,2048]{2,1,0:T(8,128)(2,1)S(1)} %bitcast.232), kind=kOutput, calls=%fused_computation.34 | convolution fusion | flops 10741612544 | bytes 18874368 | tf_op jit(solution)/shard_map/dot_general | solution.py:109
  772.5 71.0 %reduce-scatter.2.cloned.1.call-done = bf16[8,64,2048]{2,1,0:T(8,128)(2,1)} async-done(((bf16[32,64,2048]{2,1,0:T(8,128)(2,1)}), bf16[8,64,2048]{2,1,0:T(8,128)(2,1)}) %reduce-scatter.2.cloned.1.call-update) | async-done | bytes 2097168 | tf_op jit(solution)/shard_map/reduce_scatter | solution.py:183
  843.5 5.7 all-to-all-start.6
  849.5 45.4 %all-to-all-done.6 = bf16[8,64,2048]{2,1,0:T(8,128)(2,1)S(1)} async-done(((bf16[8,64,2048]{2,1,0:T(8,128)(2,1)}), bf16[8,64,2048]{2,1,0:T(8,128)(2,1)S(1)}, u32[]{:S(2)}, u32[]{:S(2)}) %all-to-all-start.6) | async-done | bytes 2097184 | tf_op jit(solution)/shard_map/all_to_all | solution.py:186
  899.5 3.3 multiply_reduce_fusion
  (265 shorter events, 161.9 us)
Async XLA Ops:
  6.5 587.4 %copy-start = (f32[128]{0:T(128)S(1)}, f32[128]{0:T(128)}, u32[]{:S(2)}) copy-start(f32[128]{0:T(128)} %param.24) | copy-start | bytes 1540
  7.8 21.1 %all-to-all-start.1 = ((bf16[8,2,128]{2,1,0:T(2,128)(2,1)}), bf16[8,2,128]{2,1,0:T(2,128)(2,1)S(1)}, u32[]{:S(2)}, u32[]{:S(2)}) async-start(bf16[8,2,128]{2,1,0:T(2,128)(2,1)} %bitcast.173), calls=%async_computation.1 | async-start | bytes 8192 | tf_op jit(solution)/shard_map/all_to_all | solution.py:133
  15.9 19.1 %copy-start.14 = (f32[1,2,1024]{2,1,0:T(2,128)S(1)}, f32[1,2,1024]{2,1,0:T(2,128)}, u32[]{:S(2)}) copy-start(f32[1,2,1024]{2,1,0:T(2,128)} %param.23) | copy-start | bytes 24580
  15.9 20.8 %copy-start.20 = (s32[1,128,2]{1,2,0:T(2,128)S(1)}, s32[1,128,2]{1,2,0:T(2,128)}, u32[]{:S(2)}) copy-start(s32[1,128,2]{1,2,0:T(2,128)} %param.27) | copy-start | bytes 3076
  15.9 22.4 %copy-start.7 = (bf16[1,128,2048]{2,1,0:T(8,128)(2,1)S(1)}, bf16[1,128,2048]{2,1,0:T(8,128)(2,1)}, u32[]{:S(2)}) copy-start(bf16[1,128,2048]{2,1,0:T(8,128)(2,1)} %param.20) | copy-start | bytes 1572868
  28.9 38.8 %all-to-all-start = ((bf16[8,2,16384]{2,1,0:T(2,128)(2,1)}), bf16[8,2,16384]{2,1,0:T(2,128)(2,1)S(1)}, u32[]{:S(2)}, u32[]{:S(2)}) async-start(bf16[8,2,16384]{2,1,0:T(2,128)(2,1)} %reshape.251), calls=%async_computation | async-start | bytes 1048576 | tf_op jit(solution)/shard_map/all_to_all | solution.py:131
  38.2 13.3 %copy-start.8 = (bf16[1,128,2048]{2,1,0:T(8,128)(2,1)S(1)}, bf16[1,128,2048]{2,1,0:T(8,128)(2,1)}, u32[]{:S(2)}) copy-start(bf16[1,128,2048]{2,1,0:T(8,128)(2,1)} %param.18) | copy-start | bytes 1572868
  51.5 13.2 %copy-start.10 = (bf16[1,128,2048]{2,1,0:T(8,128)(2,1)S(1)}, bf16[1,128,2048]{2,1,0:T(8,128)(2,1)}, u32[]{:S(2)}) copy-start(bf16[1,128,2048]{2,1,0:T(8,128)(2,1)} %param.21) | copy-start | bytes 1572868
  67.7 17.0 %all-to-all-start.2 = ((bf16[8,2,16384]{2,1,0:T(2,128)(2,1)}), bf16[8,2,16384]{2,1,0:T(2,128)(2,1)S(1)}, u32[]{:S(2)}, u32[]{:S(2)}) async-start(bf16[8,2,16384]{2,1,0:T(2,128)(2,1)} %reshape.255), calls=%async_computation.2 | async-start | bytes 1048576 | tf_op jit(solution)/shard_map/all_to_all | solution.py:132
  84.7 7.7 copy-start.5
  84.7 29.3 %all-to-all-start.3 = ((bf16[8,2,16384]{2,1,0:T(2,128)(2,1)}), bf16[8,2,16384]{2,1,0:T(2,128)(2,1)}, u32[]{:S(2)}, u32[]{:S(2)}) async-start(bf16[8,2,16384]{2,1,0:T(2,128)(2,1)} %reshape.257), calls=%async_computation.3 | async-start | bytes 1048576 | tf_op jit(solution)/shard_map/all_to_all | solution.py:130
  122.0 10.8 %copy-start.3 = (f32[1024,2,128]{0,2,1:T(8,128)S(1)}, f32[1024,2,128]{0,2,1:T(8,128)}, u32[]{:S(2)}) copy-start(f32[1024,2,128]{0,2,1:T(8,128)} %get-tuple-element.168) | copy-start | bytes 3145732
  137.2 4.5 copy-start.2
  141.7 4.8 copy-start.11
  141.7 4.8 copy-start.12
  141.7 4.8 copy-start.13
  141.7 4.8 copy-start.16
  141.7 4.8 copy-start.17
  467.7 2.9 copy-start.4
  581.9 10.4 %copy-start.18 = (s32[2,128]{1,0:T(2,128)S(1)}, s32[2,128]{1,0:T(2,128)}, u32[]{:S(2)}) copy-start(s32[2,128]{1,0:T(2,128)} %eq.52) | copy-start | bytes 3076
  581.9 11.6 %copy-start.19 = (s32[256]{0:T(256)S(1)}, s32[256]{0:T(256)}, u32[]{:S(2)}) copy-start(s32[256]{0:T(256)} %eq.48) | copy-start | bytes 3076
  586.8 16.6 %all-to-all-start.4 = ((bf16[8,2,16384]{2,1,0:T(2,128)(2,1)}), bf16[8,2,16384]{2,1,0:T(2,128)(2,1)S(1)}, u32[]{:S(2)}, u32[]{:S(2)}) async-start(bf16[8,2,16384]{2,1,0:T(2,128)(2,1)} %reshape.259), calls=%async_computation.4 | async-start | bytes 1048576 | tf_op jit(solution)/shard_map/all_to_all | solution.py:138
  592.2 131.5 %all-gather.2.cloned.1.call-start = ((), (), s32[]{:S(2)}) async-start(), calls=%async_computation.8 | async-start | bytes 10485760 | tf_op jit(solution)/shard_map/all_gather | solution.py:178
  604.5 1.4 copy-start.9
  605.9 4.8 copy-start.15
  662.6 180.9 %reduce-scatter.2.cloned.1.call-start = ((), (), s32[]{:S(2)}) async-start(), calls=%async_computation.9 | async-start | bytes 10485760 | tf_op jit(solution)/shard_map/reduce_scatter | solution.py:183
  723.8 16.7 %copy-start.22 = (bf16[32,64,2048]{2,1,0:T(8,128)(2,1)S(1)}, bf16[32,64,2048]{2,1,0:T(8,128)(2,1)}, u32[]{:S(2)}) copy-start(bf16[32,64,2048]{2,1,0:T(8,128)(2,1)} %all-gather.2.cloned.1.call-done) | copy-start | bytes 25165828
  723.8 33.1 %slice-start = ((s8[5242880]{0:T(1024)(128)(4,1)}), s8[4194304]{0:T(1024)(128)(4,1)S(1)}, s32[]{:S(2)}) async-start(s8[5242880]{0:T(1024)(128)(4,1)} %bitcast.231), calls=%async_computation.10 | async-start | bytes 8388608
  740.5 16.4 %slice-start.1 = ((s8[5242880]{0:T(1024)(128)(4,1)}), s8[1048576]{0:T(1024)(128)(4,1)S(1)}, s32[]{:S(2)}) async-start(s8[5242880]{0:T(1024)(128)(4,1)} %bitcast.231), calls=%async_computation.11 | async-start | bytes 2097152
  772.5 76.8 %copy-start.21 = (f32[1,128,2]{1,2,0:T(2,128)S(1)}, f32[1,128,2]{1,2,0:T(2,128)}, u32[]{:S(2)}) copy-start(f32[1,128,2]{1,2,0:T(2,128)} %param.28) | copy-start | bytes 3076
  843.5 51.4 %all-to-all-start.6 = ((bf16[8,64,2048]{2,1,0:T(8,128)(2,1)}), bf16[8,64,2048]{2,1,0:T(8,128)(2,1)S(1)}, u32[]{:S(2)}, u32[]{:S(2)}) async-start(bf16[8,64,2048]{2,1,0:T(8,128)(2,1)} %reduce-scatter.2.cloned.1.call-done), calls=%async_computation.7 | async-start | bytes 4194304 | tf_op jit(solution)/shard_map/all_to_all | solution.py:186
  899.5 4.2 copy-start.1
  (1 other events, 1.0 us)
Sparse Core Ops, SparseCore 0:
  662.7 61.0 all-gather.1
  772.6 70.8 reduce-scatter.1
where the time goes:
time: 922 us; the launch traced here: 911 us
  other arithmetic  381 us (41%)
  waiting for transfers between devices  194 us (21%)
  matrix products  164 us (18%)
  local copies, waits for them, and re-layouts  70.4 us (8%)
  blocking collectives  51.1 us (6%)
  starting transfers between devices  34.5 us (4%)
  between operations  14.3 us (2%)
    another operation x4, other arithmetic, delta_blocks(): jax.scipy.linalg.solve_triangular(system, rhs_cols, lower=True, unit_diag...  317 us
    reduce_scatter x1, waiting for transfers between devices, body(): lax.psum_scatter(partial_value.astype(jnp.bfloat16), 'dp', scatter_dimens...  71 us
    all_gather x1, waiting for transfers between devices, body(): piece = lax.all_gather(arrived, 'dp', axis=0, tiled=True)  61.2 us
    all_to_all x1, blocking collectives, body(): lax.all_to_all(outgoing, 'sp', split_axis=0, concat_axis=0, tiled=True)  51.1 us
    all_to_all x1, waiting for transfers between devices, body(): lax.all_to_all(summed, 'sp', split_axis=0, concat_axis=0, tiled=True)  45.4 us
    unnamed x6, other arithmetic  38.6 us
    dot_general x16, matrix products, advance(): jnp.einsum('nli,nif->nlf', query_inner * jnp.exp(running_total_inner)[......  31.5 us
    dot_general x16, matrix products, advance(): jnp.einsum('gbj,gbs->gjs', trailing_key, incoming_values, precision=TOP_P...  25.4 us
  transfers between devices with their start and end apart: 8, of which 5 were waited for; matrix products, arithmetic and copies ran while one was open for 8% of the time, Pallas kernels for 0%

commit v1 on v0

v1 whole, which is shorter than its diff:
```python
import functools

import jax
import jax.numpy as jnp
from jax import lax
from jax.experimental import pallas as pl
from jax.experimental.pallas import tpu as pltpu
from jax.sharding import PartitionSpec as P

HEAD_DIM = 128
CHUNK = 128
CORES = 2
EPSILON = 1e-06
MESH = pl.DeviceIdType.MESH


def mm(a, b):
    return lax.dot_general(a, b, (((1,), (0,)), ((), ())), preferred_element_type=jnp.float32)


def mm_t(a, b):
    return lax.dot_general(a, b, (((1,), (1,)), ((), ())), preferred_element_type=jnp.float32)


def mixer_kernel(
    n_heads, q_ref, k_ref, v_ref, beta_ref, rate_ref, out_ref, upd, wq, ins, trail, reads, state
):
    n_chunks = q_ref.shape[0] // CHUNK
    bf = jnp.bfloat16
    row = lax.broadcasted_iota(jnp.int32, (CHUNK, CHUNK), 0)
    col = lax.broadcasted_iota(jnp.int32, (CHUNK, CHUNK), 1)
    chains = [(head, way) for head in range(n_heads) for way in range(2)]

    def prepare(c, carry):
        rows = pl.ds(pl.multiple_of(c * CHUNK, CHUNK), CHUNK)
        apart = row ^ col
        eye = row == col
        todo = []
        for head in range(n_heads):
            lanes = slice(head * HEAD_DIM, (head + 1) * HEAD_DIM)
            q = q_ref[rows, lanes].astype(jnp.float32)
            k = k_ref[rows, lanes].astype(jnp.float32)
            v = v_ref[rows, lanes]
            qn = q * (
                lax.rsqrt(jnp.sum(q * q, axis=1, keepdims=True) + EPSILON) * HEAD_DIM ** (-0.5)
            )
            kn = k * lax.rsqrt(jnp.sum(k * k, axis=1, keepdims=True) + EPSILON)
            kn_t = kn.T
            kb = kn.astype(bf)
            gram = mm_t(kb, kb)
            cross = mm_t(qn.astype(bf), kb)
            beta_row = jax.nn.sigmoid(beta_ref[c, head : head + 1, :].astype(jnp.float32))
            rate_row = rate_ref[c, head : head + 1, :]
            beta_col = jnp.sum(jnp.where(eye, beta_row, 0.0), axis=1, keepdims=True)
            rate_col = jnp.sum(jnp.where(eye, rate_row, 0.0), axis=1, keepdims=True)
            total = jnp.sum(rate_row, axis=1, keepdims=True)
            for way in range(2):
                incl = (row >= col) if way == 0 else (row <= col)
                incl_t = (row <= col) if way == 0 else (row >= col)
                strict = (row > col) if way == 0 else (row < col)
                kept = jnp.where(incl, rate_row, 0.0)
                high = kept.astype(bf)
                low = (kept - high.astype(jnp.float32)).astype(bf)
                after = strict.astype(jnp.float32).astype(bf)
                decay = jnp.where(incl, jnp.exp(mm(high, after) + mm(low, after)), 0.0)
                run_col = jnp.sum(kept, axis=1, keepdims=True)
                run_row = jnp.sum(jnp.where(incl_t, rate_col, 0.0), axis=0, keepdims=True)
                lower = jnp.where(strict, beta_col * gram * decay, 0.0)
                inverse = jnp.where(eye, 1.0, jnp.where(apart == 1, -lower, 0.0))
                slot = (head * 2 + way) * n_chunks + c
                ins[slot] = (cross * decay).astype(bf)
                trail[slot] = (kn_t * jnp.exp(total - run_row)).astype(bf)
                wq[slot, CHUNK:, :] = (qn * jnp.exp(run_col)).astype(bf)
                todo.append([slot, lower, inverse, beta_row, jnp.exp(run_row), v, kb])
        level = 1
        while (1 << level) < CHUNK:
            firsts = []
            for item in todo:
                now = item[2].astype(bf)
                part = jnp.where((apart >> level) == 1, item[1], 0.0).astype(bf)
                firsts.append((now, mm(now, part).astype(bf)))
            for item, (now, first) in zip(todo, firsts):
                item[2] = item[2] - mm(first, now)
            level += 1
        for slot, _, inverse, beta_row, grown, v, kb in todo:
            scaled = inverse * beta_row
            upd[slot] = mm(scaled.astype(bf), v)
            wq[slot, :CHUNK, :] = mm((scaled * grown).astype(bf), kb).astype(bf)
        return carry

    lax.fori_loop(0, n_chunks, prepare, 0)
    state[...] = jnp.zeros_like(state)

    def advance(step, carry):
        work = []
        for index, (head, way) in enumerate(chains):
            c = step if way == 0 else n_chunks - 1 - step
            slot = index * n_chunks + c
            work.append((index, head, way, c, slot, mm(wq[slot], state[index].astype(bf))))
        fresh = []
        for index, head, way, c, slot, both in work:
            fresh.append((upd[slot] - both[:CHUNK]).astype(bf))
        for (index, head, way, c, slot, both), new in zip(work, fresh):
            total = jnp.sum(rate_ref[c, head : head + 1, :], axis=1, keepdims=True)
            state[index] = state[index] * jnp.exp(total) + mm(trail[slot], new)
        for (index, head, way, c, slot, both), new in zip(work, fresh):
            reads[slot] = both[CHUNK:] + mm(ins[slot], new)
        return carry

    lax.fori_loop(0, n_chunks, advance, 0)

    def finish(c, carry):
        rows = pl.ds(pl.multiple_of(c * CHUNK, CHUNK), CHUNK)
        for head in range(n_heads):
            lanes = slice(head * HEAD_DIM, (head + 1) * HEAD_DIM)
            one = reads[head * 2 * n_chunks + c]
            two = reads[(head * 2 + 1) * n_chunks + c]
            out_ref[rows, lanes] = (one + two).astype(bf)
        return carry

    lax.fori_loop(0, n_chunks, finish, 0)


def mix(q, k, v, beta, rate):
    length, width = q.shape
    n_heads = width // HEAD_DIM
    n_chunks = length // CHUNK
    slots = 2 * n_heads * n_chunks
    vmem = pl.BlockSpec(memory_space=pltpu.VMEM)
    return pl.pallas_call(
        functools.partial(mixer_kernel, n_heads),
        out_shape=jax.ShapeDtypeStruct((length, width), jnp.bfloat16),
        in_specs=[vmem] * 5,
        out_specs=vmem,
        scratch_shapes=[
            pltpu.VMEM((slots, CHUNK, HEAD_DIM), jnp.float32),
            pltpu.VMEM((slots, 2 * CHUNK, HEAD_DIM), jnp.bfloat16),
            pltpu.VMEM((slots, CHUNK, CHUNK), jnp.bfloat16),
            pltpu.VMEM((slots, HEAD_DIM, CHUNK), jnp.bfloat16),
            pltpu.VMEM((slots, CHUNK, HEAD_DIM), jnp.float32),
            pltpu.VMEM((2 * n_heads, HEAD_DIM, HEAD_DIM), jnp.float32),
        ],
        compiler_params=pltpu.CompilerParams(vmem_limit_bytes=40 * 1024 * 1024),
        cost_estimate=pl.CostEstimate(
            flops=40 * slots * CHUNK**3, bytes_accessed=8 * length * width, transcendentals=0
        ),
        name="mixer",
    )(q, k, v, beta, rate)


ANY = pl.BlockSpec(memory_space=pl.ANY)


def exchange_kernel(n, count, take, put, *refs):
    sources, targets = refs[:count], refs[count : 2 * count]
    send_sem, recv_sem, own_sem = refs[2 * count :]
    me = lax.axis_index("sp")
    barrier = pltpu.get_barrier_semaphore()
    for hop in range(1, n):
        pl.semaphore_signal(
            barrier, inc=1, device_id={"sp": lax.rem(me + hop, n)}, device_id_type=MESH
        )
    pl.semaphore_wait(barrier, n - 1)
    copies = []
    for hop in range(1, n):
        peer = lax.rem(me + hop, n)
        for i in range(count):
            copy = pltpu.make_async_remote_copy(
                src_ref=take(sources[i], peer),
                dst_ref=put(targets[i], me),
                send_sem=send_sem.at[i, hop - 1],
                recv_sem=recv_sem.at[i, hop - 1],
                device_id={"sp": peer},
                device_id_type=MESH,
            )
            copy.start()
            copies.append(copy)
    for i in range(count):
        copy = pltpu.make_async_copy(
            take(sources[i], me), put(targets[i], me), own_sem.at[i]
        )
        copy.start()
        copies.append(copy)
    for copy in copies:
        copy.wait()


def exchange(n, arrays, shapes, take, put, collective_id, name):
    count = len(arrays)
    return pl.pallas_call(
        functools.partial(exchange_kernel, n, count, take, put),
        out_shape=[jax.ShapeDtypeStruct(s, a.dtype) for s, a in zip(shapes, arrays)],
        in_specs=[ANY] * count,
        out_specs=[ANY] * count,
        scratch_shapes=[
            pltpu.SemaphoreType.DMA((count, n - 1)),
            pltpu.SemaphoreType.DMA((count, n - 1)),
            pltpu.SemaphoreType.DMA((count,)),
        ],
        compiler_params=pltpu.CompilerParams(collective_id=collective_id, has_side_effects=True),
        name=name,
    )(*arrays)


def lead_block(ref, index):
    return ref.at[index]


def row_block(rows, ref, index):
    return ref.at[pl.ds(pl.multiple_of(index * rows, rows), rows), :]


def lane_block(lanes, ref, index):
    return ref.at[:, pl.ds(pl.multiple_of(index * lanes, lanes), lanes)]


def spread_kernel(
    n, n_dp, x_ref, out_ref, own_sem, a_send, a_recv, b_send, b_recv, c_send, c_recv
):
    me, mine = lax.axis_index("sp"), lax.axis_index("dp")
    chips = n_dp // CORES
    chip, core = mine // CORES, lax.rem(mine, CORES)
    sibling = chip * CORES + (1 - core)
    barrier = pltpu.get_barrier_semaphore()
    for hop in range(1, n):
        pl.semaphore_signal(
            barrier, inc=1, device_id={"sp": lax.rem(me + hop, n)}, device_id_type=MESH
        )
    for turn in range(1, chips):
        other = lax.rem(chip + turn, chips) * CORES + core
        pl.semaphore_signal(barrier, inc=1, device_id={"dp": other}, device_id_type=MESH)
    pl.semaphore_signal(barrier, inc=1, device_id={"dp": sibling}, device_id_type=MESH)
    pl.semaphore_wait(barrier, n - 1 + chips - 1 + 1)

    own = pltpu.make_async_copy(x_ref.at[me], out_ref.at[mine, me], own_sem)
    own.start()
    first = [None]
    for hop in range(1, n):
        peer = lax.rem(me + hop, n)
        copy = pltpu.make_async_remote_copy(
            src_ref=x_ref.at[peer],
            dst_ref=out_ref.at[mine, me],
            send_sem=a_send.at[hop - 1],
            recv_sem=a_recv.at[hop - 1],
            device_id={"sp": peer},
            device_id_type=MESH,
        )
        copy.start()
        first.append(copy)
    across, beside = {}, []
    for hop in range(n):
        origin = lax.rem(me + n - hop, n)
        if hop == 0:
            block = x_ref.at[me]
        else:
            first[hop].wait_recv()
            block = out_ref.at[mine, origin]
        for turn in range(1, chips):
            other = lax.rem(chip + turn, chips) * CORES + core
            copy = pltpu.make_async_remote_copy(
                src_ref=block,
                dst_ref=out_ref.at[mine, origin],
                send_sem=b_send.at[turn - 1, hop],
                recv_sem=b_recv.at[turn - 1, hop],
                device_id={"dp": other},
                device_id_type=MESH,
            )
            copy.start()
            across[turn, hop] = copy
        copy = pltpu.make_async_remote_copy(
            src_ref=block,
            dst_ref=out_ref.at[mine, origin],
            send_sem=c_send.at[0, hop],
            recv_sem=c_recv.at[0, hop],
            device_id={"dp": sibling},
            device_id_type=MESH,
        )
        copy.start()
        beside.append(copy)
    for hop in range(n):
        origin = lax.rem(me + n - hop, n)
        for turn in range(1, chips):
            across[turn, hop].wait_recv()
            giver = lax.rem(chip + chips - turn, chips) * CORES + core
            copy = pltpu.make_async_remote_copy(
                src_ref=out_ref.at[giver, origin],
                dst_ref=out_ref.at[giver, origin],
                send_sem=c_send.at[turn, hop],
                recv_sem=c_recv.at[turn, hop],
                device_id={"dp": sibling},
                device_id_type=MESH,
            )
            copy.start()
            beside.append(copy)
    own.wait()
    for hop in range(1, n):
        first[hop].wait_send()
    for copy in across.values():
        copy.wait_send()
    for copy in beside:
        copy.wait()


def spread(n, n_dp, x, collective_id):
    chips = n_dp // CORES
    dma = pltpu.SemaphoreType.DMA
    return pl.pallas_call(
        functools.partial(spread_kernel, n, n_dp),
        out_shape=jax.ShapeDtypeStruct((n_dp,) + x.shape, x.dtype),
        in_specs=[ANY],
        out_specs=ANY,
        scratch_shapes=[
            dma,
            dma((n - 1,)),
            dma((n - 1,)),
            dma((max(chips - 1, 1), n)),
            dma((max(chips - 1, 1), n)),
            dma((chips, n)),
            dma((chips, n)),
        ],
        compiler_params=pltpu.CompilerParams(collective_id=collective_id, has_side_effects=True),
        name="spread",
    )(x)


def expert_part(rows, gate_local, up_local, down_local):
    gate_act = jnp.dot(rows, gate_local, preferred_element_type=jnp.float32)
    up_act = jnp.dot(rows, up_local, preferred_element_type=jnp.float32)
    hidden = (jax.nn.silu(gate_act) * up_act).astype(jnp.bfloat16)
    return jnp.dot(hidden, down_local, preferred_element_type=jnp.float32)


def body(
    stream,
    query_proj,
    key_proj,
    value_proj,
    out_gate,
    beta_logit,
    log_decay,
    head_gain,
    out_proj,
    ffn_gain,
    routes,
    route_weight,
    expert_gate,
    expert_up,
    expert_down,
):
    n_sp = lax.axis_size("sp")
    n_dp = lax.axis_size("dp")
    tok_here = stream.shape[1]
    heads_here = log_decay.shape[1]
    length = log_decay.shape[2]
    width = heads_here * HEAD_DIM
    beta_out = beta_logit[0].T.astype(jnp.float32).reshape(n_sp, heads_here, tok_here)
    beta_out = jnp.pad(beta_out, ((0, 0), (0, -heads_here % 8), (0, 0)))
    projections = exchange(
        n_sp,
        (query_proj[0], key_proj[0], value_proj[0]),
        ((length, width),) * 3,
        functools.partial(lane_block, width),
        functools.partial(row_block, tok_here),
        1,
        "to_heads",
    )
    (beta_in,) = exchange(
        n_sp, (beta_out,), (beta_out.shape,), lead_block, lead_block, 2, "to_heads_beta"
    )
    pieces = tok_here // CHUNK
    beta_in = beta_in[:, :heads_here].reshape(n_sp, heads_here, pieces, CHUNK)
    beta_in = beta_in.transpose(0, 2, 1, 3).reshape(n_sp * pieces, heads_here, CHUNK)
    rate_in = log_decay[0].reshape(heads_here, length // CHUNK, CHUNK).transpose(1, 0, 2)
    mixed = mix(*projections, beta_in, rate_in)
    (tokens_view,) = exchange(
        n_sp,
        (mixed,),
        ((tok_here, n_sp * width),),
        functools.partial(row_block, tok_here),
        functools.partial(lane_block, width),
        3,
        "to_tokens",
    )
    tok_count = stream.shape[1]
    model_width = stream.shape[2]
    n_heads = tokens_view.shape[1] // HEAD_DIM
    per_head = tokens_view.astype(jnp.float32).reshape(tok_count, n_heads, HEAD_DIM)
    normed_heads = (
        per_head
        * lax.rsqrt(jnp.mean(per_head * per_head, axis=-1, keepdims=True) + EPSILON)
        * head_gain
    )
    gated = (
        normed_heads.reshape(tok_count, -1) * jax.nn.silu(out_gate[0].astype(jnp.float32))
    ).astype(jnp.bfloat16)
    resid = stream[0].astype(jnp.float32) + jnp.dot(
        gated, out_proj, preferred_element_type=jnp.float32
    )
    ffn_in = (
        resid * lax.rsqrt(jnp.mean(resid * resid, axis=-1, keepdims=True) + EPSILON) * ffn_gain
    ).astype(jnp.bfloat16)
    top_count = routes.shape[2]
    capacity = tok_count * top_count * 2 // n_sp
    flat_routes = routes.reshape(-1)
    expert_ids = lax.broadcasted_iota(jnp.int32, (1, n_sp), 1)
    chosen = (flat_routes[:, None] == expert_ids).astype(jnp.int32)
    earlier = jnp.cumsum(chosen, axis=0) - chosen
    slot_ids = flat_routes * capacity + jnp.sum(earlier * chosen, axis=1)
    slot_grid = lax.broadcasted_iota(jnp.int32, (n_sp * capacity, 1), 0)
    placing = (
        (slot_grid == slot_ids[None, :])
        .astype(jnp.int32)
        .reshape(n_sp * capacity, tok_count, top_count)
    )
    placing = jnp.sum(placing, axis=2).astype(jnp.bfloat16)
    outgoing = jnp.dot(placing, ffn_in, preferred_element_type=jnp.float32).astype(jnp.bfloat16)
    outgoing = outgoing.reshape(n_sp, capacity, model_width)
    gate_local = expert_gate[0]
    up_local = expert_up[0]
    down_local = expert_down[0]
    piece = spread(n_sp, n_dp, outgoing, 4)
    flat_rows = piece.reshape(-1, model_width)
    partial_value = expert_part(flat_rows, gate_local, up_local, down_local).reshape(
        n_dp * n_sp, capacity, model_width
    )
    summed = lax.psum_scatter(
        partial_value.astype(jnp.bfloat16), "dp", scatter_dimension=0, tiled=True
    )
    (returned,) = exchange(
        n_sp, (summed,), (summed.shape,), lead_block, lead_block, 5, "expert_return"
    )
    picked = returned.reshape(n_sp * capacity, model_width)[slot_ids]
    picked = picked.reshape(tok_count, top_count, model_width).astype(jnp.float32)
    routed = jnp.sum(picked * route_weight[0][..., None], axis=1)
    return (resid + routed).astype(jnp.bfloat16)[None]


def solution(mesh):
    return jax.shard_map(
        body,
        mesh=mesh,
        in_specs=(
            P("dp", "sp", None),
            P("dp", "sp", None),
            P("dp", "sp", None),
            P("dp", "sp", None),
            P("dp", "sp", None),
            P("dp", "sp", None),
            P("dp", "sp", None),
            P(),
            P(),
            P(),
            P("dp", "sp", None),
            P("dp", "sp", None),
            P("sp", None, "dp"),
            P("sp", None, "dp"),
            P("sp", "dp", None),
        ),
        out_specs=P("dp", "sp", None),
        check_vma=False,
    )
```

time: 922 us -> 366 us (0.40); the launches traced: 911 us -> 366 us
  other arithmetic: 381 us -> 9.11 us
  Pallas kernels: 0 us -> 192 us
  waiting for transfers between devices: 194 us -> 81.6 us
  matrix products: 164 us -> 55.8 us
  local copies, waits for them, and re-layouts: 70.4 us -> 13.9 us
  blocking collectives: 51.1 us -> 0 us
  starting transfers between devices: 34.5 us -> 0.01 us
    another operation x7 -> x2, other arithmetic: 319 us -> 0.62 us  [the longest x4 317 us: delta_blocks(): jax.scipy.linalg.solve_triangular(system, rhs_cols, lower=True, unit_diag...]
    pallas_call x0 -> x6, Pallas kernels: none -> 192 us  [the longest x4 109 us: exchange(): pl.pallas_call(functools.partial(exchange_kernel, n, count, take, put), o...]
    dot_general x66 -> x0, matrix products: 106 us -> none  [the longest x16 31.5 us: advance(): jnp.einsum('nli,nif->nlf', query_inner * jnp.exp(running_total_inner)[......]
    all_to_all x6 -> x0, waiting for transfers between devices: 62.1 us -> none  [the longest x1 45.4 us: body(): lax.all_to_all(summed, 'sp', split_axis=0, concat_axis=0, tiled=True)]
    all_gather x1 -> x0, waiting for transfers between devices: 61.2 us -> none  [body(): piece = lax.all_gather(arrived, 'dp', axis=0, tiled=True)]
    all_to_all x1 -> x0, blocking collectives: 51.1 us -> none  [body(): lax.all_to_all(outgoing, 'sp', split_axis=0, concat_axis=0, tiled=True)]
    unnamed x6 -> x2, other arithmetic: 38.6 us -> 1.21 us
    all_to_all x6 -> x0, starting transfers between devices: 34.5 us -> none  [the longest x1 6.07 us: body(): lax.all_to_all(query_proj, 'sp', split_axis=2, concat_axis=1, tiled=True)]
  transfers between devices with their start and end apart: 8 -> 1, of which waited for: 5 -> 1; matrix products, arithmetic and copies ran while one was open for 8% -> 0% of each run, Pallas kernels for 0% -> 0%
where the time goes in v1:
time: 366 us
  Pallas kernels  192 us (52%)
  waiting for transfers between devices  81.6 us (22%)
  matrix products  55.8 us (15%)
  local copies, waits for them, and re-layouts  13.9 us (4%)
  between operations  13.7 us (4%)
  other arithmetic  9.11 us (2%)
    pallas_call x4, Pallas kernels, exchange(): pl.pallas_call(functools.partial(exchange_kernel, n, count, take, put), o...  109 us
    reduce_scatter x1, waiting for transfers between devices, body(): lax.psum_scatter(partial_value.astype(jnp.bfloat16), 'dp', scatter_dimens...  81.6 us
    pallas_call x1, Pallas kernels, spread(): pl.pallas_call(functools.partial(spread_kernel, n, n_dp), out_shape=jax.S...  62.9 us
    pallas_call x1, Pallas kernels, mix(): pl.pallas_call(functools.partial(mixer_kernel, n_heads), out_shape=jax.Sh...  20.1 us
    dot_general x1, matrix products, expert_part(): gate_act = jnp.dot(rows, gate_local, preferred_element_type=jnp.float32)  16.7 us
    dot_general x1, matrix products, expert_part(): return jnp.dot(hidden, down_local, preferred_element_type=jnp.float32)  16.6 us
    dot_general x1, matrix products, expert_part(): up_act = jnp.dot(rows, up_local, preferred_element_type=jnp.float32)  15.1 us
  transfers between devices with their start and end apart: 1, of which 1 were waited for; matrix products, arithmetic and copies ran while one was open for 0% of the time, Pallas kernels for 0%

profile of v1, /device:TPU:13, one launch (start us, length us, event | category | flops | bytes accessed | tf_op | source)
XLA Modules:
  0.0 365.7 jit_solution(4722902254134361410)
XLA Ops:
  6.5 0.8 copy.35
  7.6 1.3 pad_convert_fusion.refs_0_
  8.9 6.2 %to_heads_beta.1 = f32[8,8,128]{2,1,0:T(8,128)} custom-call(f32[8,8,128]{2,1,0:T(8,128)} %pad_convert_fusion.refs_0_), custom_call_target="tpu_custom_call" | custom-call | tf_op jit(solution)/shard_map/to_heads_beta/pallas_call | solution.py:190
  15.1 0.8 slice.9.beta_ref
  15.9 38.5 %to_heads.1 = (bf16[1024,256]{1,0:T(8,128)(2,1)}, bf16[1024,256]{1,0:T(8,128)(2,1)}, bf16[1024,256]{1,0:T(8,128)(2,1)}) custom-call(bf16[128,2048]{1,0:T(8,128)(2,1)} %bitcast.73, bf16[128,2048]{1,0:T(8,128)(2,1)} %bitcast.74, bf16[128,2048]{1,0:T(8,128)(2,1)} %bitcast.75), custom_call_target="tpu_custom_call" | custom-call | tf_op jit(solution)/shard_map/to_heads/pallas_call | solution.py:190
  54.4 1.0 copy-done.3
  55.4 1.0 copy-done.4
  56.4 1.0 copy-done.5
  57.5 0.7 copy-done.6
  58.2 20.1 %mixer.1.refs_0_ = bf16[1024,256]{1,0:T(8,128)(2,1)S(1)} custom-call(bf16[1024,256]{1,0:T(8,128)(2,1)S(1)} %copy-done.3, bf16[1024,256]{1,0:T(8,128)(2,1)S(1)} %copy-done.4, bf16[1024,256]{1,0:T(8,128)(2,1)S(1)} %copy-done.5, f32[8,2,128]{2,1,0:T(2,128)S(1)} %slice.9.beta_ref, f32[8,2,128]{2,1,0:T(2,128)S(1)} %bitcast.66), custom_call_target="tpu_custom_call" | custom-call | flops 2684354560 | bytes 2097152 | tf_op jit(solution)/shard_map/mixer/pallas_call | solution.py:130
  78.3 0.8 copy-done.2
  79.1 14.0 %to_tokens.1 = bf16[128,2048]{1,0:T(8,128)(2,1)} custom-call(bf16[1024,256]{1,0:T(8,128)(2,1)} %copy-done.2), custom_call_target="tpu_custom_call" | custom-call | tf_op jit(solution)/shard_map/to_tokens/pallas_call | solution.py:190
  93.1 1.2 fusion.4
  94.4 0.2 copy.40
  94.5 0.3 reduce_sum.49
  95.1 0.3 mul.101
  95.5 5.2 %multiply_reduce_fusion.1 = (f32[128]{0:T(128)S(1)}, f32[128,2048]{1,0:T(8,128)S(1)}) fusion(bf16[2048,2048]{1,0:T(8,128)(2,1)} %param.23, bf16[128,2048]{1,0:T(8,128)(2,1)S(1)} %copy-done.9, f32[16,8,16,128]{3,2,1,0:T(8,128)S(1)} %bitcast.72, bf16[1,128,2048]{2,1,0:T(8,128)(2,1)S(1)} %copy-done.12, f32[2048]{0:T(1024)S(1)} %broadcast_bitcast_fusion, ...), kind=kOutput, calls=%fused_computation.23 | convolution fusion | flops 1077411712 | bytes 12067328 | tf_op jit(solution)/shard_map/dot_general | solution.py:396
  100.7 0.6 reduce-window.6
  101.3 0.2 slice_reduce_fusion
  101.7 0.1 reduce_sum.51
  102.0 2.1 convolution_convert_fusion.1
  104.1 62.9 %spread.1 = bf16[4,8,64,2048]{3,2,1,0:T(8,128)(2,1)} custom-call(bf16[8,64,2048]{2,1,0:T(8,128)(2,1)} %bitcast.70), custom_call_target="tpu_custom_call" | custom-call | tf_op jit(solution)/shard_map/spread/pallas_call | solution.py:307
  167.1 16.7 %fusion.2 = f32[2048,1280]{1,0:T(8,128)} fusion(bf16[2048,2048]{1,0:T(8,128)(2,1)} %bitcast.68, bf16[1,2048,1280]{2,1,0:T(8,128)(2,1)} %param.27), kind=kOutput, calls=%fused_computation.5 | convolution fusion | flops 10737418240 | bytes 24117248 | tf_op jit(solution)/shard_map/dot_general | solution.py:327
  183.8 15.1 %multiply_convert_fusion = bf16[2048,1280]{1,0:T(8,128)(2,1)} fusion(f32[2048,1280]{1,0:T(8,128)} %fusion.2, bf16[2048,2048]{1,0:T(8,128)(2,1)S(1)} %bitcast.69, bf16[1,2048,1280]{2,1,0:T(8,128)(2,1)S(1)} %bitcast.81), kind=kOutput, calls=%fused_computation.1 | convolution fusion | flops 10753146880 | bytes 29360128 | tf_op jit(solution)/shard_map/dot_general | solution.py:328
  198.9 16.6 %convolution_convert_fusion = bf16[32,64,2048]{2,1,0:T(8,128)(2,1)} fusion(bf16[32,64,1280]{2,1,0:T(8,128)(2,1)} %bitcast.82, bf16[1,1280,2048]{2,1,0:T(8,128)(2,1)} %param.29), kind=kOutput, calls=%fused_computation.2 | convolution fusion | flops 10741612544 | bytes 18874368 | tf_op jit(solution)/shard_map/dot_general | solution.py:330
  215.7 0.5 copy-done.11
  216.3 81.6 %reduce-scatter.2.cloned.1.call-done.refs_0_ = bf16[8,64,2048]{2,1,0:T(8,128)(2,1)} async-done(((bf16[32,64,2048]{2,1,0:T(8,128)(2,1)}), bf16[8,64,2048]{2,1,0:T(8,128)(2,1)}) %reduce-scatter.2.cloned.1.call-update) | async-done | bytes 2097168 | tf_op jit(solution)/shard_map/reduce_scatter | solution.py:426
  298.0 49.9 %expert_return.1 = bf16[8,64,2048]{2,1,0:T(8,128)(2,1)} custom-call(bf16[8,64,2048]{2,1,0:T(8,128)(2,1)} %reduce-scatter.2.cloned.1.call-done.refs_0_), custom_call_target="tpu_custom_call" | custom-call | tf_op jit(solution)/shard_map/expert_return/pallas_call | solution.py:190
  347.9 4.2 %gather_fusion = bf16[256,2048]{1,0:T(8,128)(2,1)S(1)} fusion(bf16[512,2048]{1,0:T(8,128)(2,1)} %bitcast.67, s32[1024]{0:T(1024)S(1)} %pad_clamp_fusion), kind=kCustom, calls=%fused_computation | custom fusion | bytes 2098176 | tf_op jit(solution)/shard_map/gather | solution.py:432
  352.1 1.3 reshape.121
  353.4 3.3 multiply_reduce_fusion
  356.7 2.1 fusion.11
  (48 shorter events, 1.1 us)
Async XLA Ops:
  6.5 88.5 %copy-start = (f32[128]{0:T(128)S(1)}, f32[128]{0:T(128)}, u32[]{:S(2)}) copy-start(f32[128]{0:T(128)} %param.22) | copy-start | bytes 1540
  6.5 291.4 %reduce-scatter.2.cloned.1.call-start = ((), (), s32[]{:S(2)}) async-start(), calls=%async_computation.1 | async-start | bytes 10485760 | tf_op jit(solution)/shard_map/reduce_scatter | solution.py:426
  54.3 1.0 copy-start.3
  55.4 1.0 copy-start.4
  56.4 1.0 copy-start.5
  57.5 0.7 copy-start.6
  78.3 0.8 copy-start.2
  79.1 16.4 %copy-start.12 = (bf16[1,128,2048]{2,1,0:T(8,128)(2,1)S(1)}, bf16[1,128,2048]{2,1,0:T(8,128)(2,1)}, u32[]{:S(2)}) copy-start(bf16[1,128,2048]{2,1,0:T(8,128)(2,1)} %param.19) | copy-start | bytes 1572868
  79.1 16.4 %copy-start.13 = (bf16[1,128,2048]{2,1,0:T(8,128)(2,1)S(1)}, bf16[1,128,2048]{2,1,0:T(8,128)(2,1)}, u32[]{:S(2)}) copy-start(bf16[1,128,2048]{2,1,0:T(8,128)(2,1)} %param.15) | copy-start | bytes 1572868
  93.1 2.3 copy-start.9
  95.5 6.5 %copy-start.10 = (f32[2048]{0:T(1024)S(1)}, f32[2048]{0:T(1024)}, u32[]{:S(2)}) copy-start(f32[2048]{0:T(1024)} %param.24) | copy-start | bytes 24580
  100.7 66.4 %copy-start.8 = (f32[128,2048]{1,0:T(8,128)}, f32[128,2048]{1,0:T(8,128)S(1)}, u32[]{:S(2)}) copy-start(f32[128,2048]{1,0:T(8,128)S(1)} %get-tuple-element.12) | copy-start | bytes 3145732
  104.1 79.7 %slice-start = ((s8[5242880]{0:T(1024)(128)(4,1)}), s8[1048576]{0:T(1024)(128)(4,1)S(1)}, s32[]{:S(2)}) async-start(s8[5242880]{0:T(1024)(128)(4,1)} %bitcast.80), calls=%async_computation.2 | async-start | bytes 2097152
  167.0 16.8 %copy-start.7 = (bf16[4,8,64,2048]{3,2,1,0:T(8,128)(2,1)S(1)}, bf16[4,8,64,2048]{3,2,1,0:T(8,128)(2,1)}, u32[]{:S(2)}) copy-start(bf16[4,8,64,2048]{3,2,1,0:T(8,128)(2,1)} %spread.1) | copy-start | bytes 25165828
  167.1 16.8 %slice-start.1 = ((s8[5242880]{0:T(1024)(128)(4,1)}), s8[4194304]{0:T(1024)(128)(4,1)S(1)}, s32[]{:S(2)}) async-start(s8[5242880]{0:T(1024)(128)(4,1)} %bitcast.80), calls=%async_computation.3 | async-start | bytes 8388608
  215.5 0.7 copy-start.11
  347.9 11.0 %copy-start.1 = (f32[128]{0:T(128)S(1)}, f32[128]{0:T(128)}, u32[]{:S(2)}) copy-start(f32[128]{0:T(128)} %param.22) | copy-start | bytes 1540
Sparse Core Ops, SparseCore 0:
  215.7 82.2 reduce-scatter.1
